TPU v7x, 32 devices: a whole 2x2x4 slice. The times are simulated.
32 devices in a mesh: grp: 2 (over y), sp: 4 (over z), tp: 4 (over x, core).
Axes of the slice: x: 2, y: 2, z: 4, core: 2. Of those that a mesh axis runs over, the one named last changes fastest.
Arguments:
- stream: bfloat16 [2048, 2048], P(('grp', 'sp'), 'tp'), parts along dimension 0, may hold values from -1.5 to 1.5
- layer_norm_gain: float32 [2, 2048], replicated, may hold values from 0.1 to 1.9
- convolution_in_weight: bfloat16 [2, 2048, 1536], P(None, 'sp', 'tp'), may hold values from -0.125 to 0.125
- gating_in_weight: bfloat16 [2, 2048, 1536], P(None, 'sp', 'tp'), may hold values from -0.125 to 0.125
- output_weight: bfloat16 [2, 1536, 2048], P(None, 'tp', 'sp'), may hold values from -0.15625 to 0.15625
- convolution_kernel_taps: float32 [2, 4, 1536], P(None, None, 'tp'), may hold values from -12 to 12
- recurrent_gate_blocks: bfloat16 [2, 2, 2, 12, 128, 128], P(None, None, None, 'tp'), may hold values from -0.5 to 0.5
- channel_decay_logit: float32 [2, 2, 1536], P(None, None, 'tp')
- position_decay_boost: float32 [2, 2, 2048], P(None, None, ('grp', 'sp')), parts along dimension 2, may hold values from -1.4 to 0, as said below
Outputs:
- new_stream: bfloat16 [2048, 2048], P(('grp', 'sp'), 'tp'), parts along dimension 0
There are 2 independent parts, one for each index of `grp`. A program takes and returns all parts, laid end to end along the dimension named above; an argument that names none is the same for every part. Nothing has to cross between parts.
Inputs may be any that keep to these rules, and one draw needn't show every extreme that they name: `position_decay_boost`: zero at all but a few positions.
All inputs are finite; a program needn't handle non-finite values.
Results may differ from a plain program's by a relative error of at most 0.025.
Values may be sent and summed in bfloat16 or wider, within the bound.
A program may use at most 128 MiB of HBM per device.

v0:
```python
import functools

import jax
import jax.numpy as jnp
from jax import lax
from jax.experimental import pallas as pl
from jax.experimental.pallas import tpu as pltpu
from jax.sharding import PartitionSpec as P

EPS = 1e-06
RECURRENT_WIDTH = 8.0
TILE = 16
HALO = 8
MESH = pl.DeviceIdType.MESH


def own_share(rows, n_grp):
    if n_grp != 2:
        return rows
    return min(rows, -(-rows * 11 // (20 * TILE)) * TILE)


def one_minus_square(log_decay, decay):
    y = 2.0 * log_decay
    series = y * (1 / 720) + 1 / 120
    series = series * y + 1 / 24
    series = series * y + 1 / 6
    series = series * y + 0.5
    series = series * y + 1.0
    return jnp.where(y > -0.25, -y * series, 1.0 - decay * decay)


def scanned(a, b, reverse):
    count = a.shape[0]
    row = lax.broadcasted_iota(jnp.int32, a.shape, 0)
    step = 1
    while step < count:
        inside = row < count - step if reverse else row >= step
        shift = count - step if reverse else step
        a_near = jnp.where(inside, pltpu.roll(a, shift, 0), 1.0)
        b_near = jnp.where(inside, pltpu.roll(b, shift, 0), 0.0)
        b = a * b_near + b
        a = a * a_near
        step *= 2
    return a, b


def kernel(
    n_grp, n_sp, n_tp,
    stream, gain, conv_w, gate_w, out_w, taps, blocks, rate, boost,
    out,
    full, normed, g_in, g_out, xpad, y_act, cum, loc, ends, gated, parts, sums,
    z_send, z_recv, y_send, y_recv, f_send, f_recv, r_send, r_recv,
    h_send, h_recv, e_send, e_recv,
):
    g, s, t = lax.axis_index("grp"), lax.axis_index("sp"), lax.axis_index("tp")
    layers = conv_w.shape[0]
    rows, ds = stream.shape
    cs, channels = conv_w.shape[1], conv_w.shape[2]
    width = blocks.shape[-1]
    weights = 3 * layers

    def remote(src, dst, send, recv, axis, place):
        return pltpu.make_async_remote_copy(
            src_ref=src, dst_ref=dst, send_sem=send, recv_sem=recv,
            device_id={axis: place}, device_id_type=MESH,
        )

    barrier = pltpu.get_barrier_semaphore()
    total = 0
    for axis, me, count in (("sp", s, n_sp), ("tp", t, n_tp), ("grp", g, n_grp)):
        for d in range(1, count):
            pl.semaphore_signal(
                barrier, inc=1, device_id={axis: lax.rem(me + d, count)}, device_id_type=MESH
            )
            total += 1
    pl.semaphore_wait(barrier, total)

    def mine(w):
        return (conv_w, gate_w, out_w)[w % 3].at[w // 3]

    def hold(w, c):
        return g_out.at[w // 3, c] if w % 3 == 2 else g_in.at[w // 3 * 2 + w % 3, c]

    def depth(w):
        return channels if w % 3 == 2 else cs

    def z_rows(w):
        share = own_share(depth(w), n_grp)
        if share == depth(w):
            return pl.ds(0, share)
        return pl.ds(pl.multiple_of(g * (depth(w) - share), TILE), share)

    def y_rows(w, place):
        share = own_share(depth(w), n_grp)
        return pl.ds(pl.multiple_of(place * share, TILE), depth(w) - share)

    def z_copy(w, c, src, to, slot):
        return remote(
            src.at[z_rows(w)], hold(w, c).at[z_rows(w)],
            z_send.at[w, slot], z_recv.at[w, c], "sp", to,
        )

    shared = n_grp == 2

    def y_copy(w, c, place):
        return remote(
            hold(w, c).at[y_rows(w, place)], hold(w, c).at[y_rows(w, place)],
            y_send.at[w, c], y_recv.at[w, c], "grp", 1 - g,
        )

    def has_y(w):
        return shared and own_share(depth(w), n_grp) < depth(w)

    def start_own(w):
        @pl.when(s < n_sp - 1)
        def _():
            z_copy(w, s, mine(w), s + 1, s).start()

        @pl.when(s > 0)
        def _():
            z_copy(w, s, mine(w), s - 1, n_sp).start()

    def pass_on(w, c, onward, to, back):
        z_copy(w, c, hold(w, c), back, c).wait_recv()

        @pl.when(onward)
        def _():
            z_copy(w, c, hold(w, c), to, c).start()

        if has_y(w):
            y_copy(w, c, g).start()

    def event(w, k):
        @pl.when(s - 1 - k >= 0)
        def _():
            pass_on(w, s - 1 - k, s < n_sp - 1, s + 1, s - 1)

        @pl.when(s + 1 + k <= n_sp - 1)
        def _():
            pass_on(w, s + 1 + k, s > 0, s - 1, s + 1)

        if k == 0 and w + 2 < weights:
            start_own(w + 2)

    queue = [(w, k) for w in range(weights) for k in range(n_sp - 1)]

    def serve(count):
        for _ in range(min(count, len(queue))):
            event(*queue.pop(0))

    def serve_until(w):
        while queue and queue[0][0] <= w:
            event(*queue.pop(0))

    def landed(w):
        if has_y(w):
            for c in range(n_sp):
                @pl.when(c != s)
                def _():
                    y_copy(w, c, 1 - g).wait_recv()

    def f_copy(layer, src, source, d, to):
        return remote(
            src, full.at[layer, source], f_send.at[layer, d], f_recv.at[layer, source], "tp", to
        )

    tp_order = [d for d in range(1, n_tp)]

    def send_features(layer, src):
        for d in tp_order:
            f_copy(layer, src, t, d, lax.rem(t + d, n_tp)).start()

    send_features(0, stream)
    for w in range(min(2, weights)):
        start_own(w)
    full[0, t] = stream[...]
    for w in range(weights):
        if w % 3 == 2:
            g_out[w // 3, s] = out_w[w // 3]
        else:
            g_in[w // 3 * 2 + w % 3, s] = (conv_w, gate_w)[w % 3][w // 3]

    row = lax.broadcasted_iota(jnp.int32, (rows, 1), 0)

    for layer in range(layers):
        if layer == 0:
            serve(1)
        for d in tp_order:
            source = lax.rem(t + d, n_tp)
            f_copy(layer, full.at[layer, source], source, d, source).wait_recv()
        square = jnp.zeros((rows, 1), jnp.float32)
        for j in range(n_tp):
            x = full[layer, j].astype(jnp.float32)
            square += jnp.sum(x * x, axis=-1, keepdims=True)
        inverse = lax.rsqrt(square / (n_tp * ds) + EPS)
        piece = min(cs, ds)
        for p in range(n_tp * ds // piece):
            at = p * piece
            x = full[layer, at // ds, :, at % ds : at % ds + piece].astype(jnp.float32)
            x = x * inverse * gain[layer : layer + 1, at : at + piece]
            normed[at // cs, :, at % cs : at % cs + piece] = x.astype(jnp.bfloat16)

        def project(w):
            acc = None
            for c in range(n_sp):
                term = jnp.dot(
                    normed[c], g_in[w // 3 * 2 + w % 3, c], preferred_element_type=jnp.float32
                )
                acc = term if acc is None else acc + term
            return acc.astype(jnp.bfloat16).astype(jnp.float32)

        wx, wy, wo = 3 * layer, 3 * layer + 1, 3 * layer + 2
        serve_until(wx)
        if layer == 0:
            serve(1)
        landed(wx)
        xpad[layer, HALO : HALO + rows] = project(wx)

        def halo_right():
            return remote(
                xpad.at[layer, pl.ds(rows, HALO)], xpad.at[layer, pl.ds(0, HALO)],
                h_send.at[layer, 0], h_recv.at[layer, 0], "sp", lax.rem(s + 1, n_sp),
            )

        def halo_left():
            return remote(
                xpad.at[layer, pl.ds(HALO, HALO)], xpad.at[layer, pl.ds(HALO + rows, HALO)],
                h_send.at[layer, 1], h_recv.at[layer, 1], "sp", lax.rem(s + n_sp - 1, n_sp),
            )

        @pl.when(s < n_sp - 1)
        def _():
            halo_right().start()

        @pl.when(s > 0)
        def _():
            halo_left().start()

        serve_until(wy)
        landed(wy)
        y_act[...] = jax.nn.gelu(project(wy))

        @pl.when(s > 0)
        def _():
            halo_right().wait_recv()

        @pl.when(s == 0)
        def _():
            xpad[layer, 0:HALO] = jnp.zeros((HALO, channels), jnp.float32)

        @pl.when(s < n_sp - 1)
        def _():
            halo_left().wait_recv()

        @pl.when(s == n_sp - 1)
        def _():
            xpad[layer, HALO + rows : 2 * HALO + rows] = jnp.zeros((HALO, channels), jnp.float32)

        for n in range(channels // width):
            lanes = slice(n * width, (n + 1) * width)
            conv = None
            for k in range(taps.shape[1]):
                term = taps[layer, k : k + 1, lanes] * xpad[
                    layer, HALO - 1 + k : HALO - 1 + k + rows, lanes
                ]
                conv = term if conv is None else conv + term
            conv_half = conv.astype(jnp.bfloat16)
            conv = conv_half.astype(jnp.float32)
            for d in range(2):
                recur = jax.nn.sigmoid(
                    jnp.dot(conv_half, blocks[layer, d, 0, n], preferred_element_type=jnp.float32)
                )
                inject = jax.nn.sigmoid(
                    jnp.dot(conv_half, blocks[layer, d, 1, n], preferred_element_type=jnp.float32)
                )
                at = 2 * layer + d
                log_decay = rate[at : at + 1, lanes] * recur + boost[:, at : at + 1]
                decay = jnp.exp(log_decay)
                first = (row == 0) & (s == 0) if d == 0 else (row == rows - 1) & (s == n_sp - 1)
                m = jnp.where(first, 1.0, jnp.sqrt(one_minus_square(log_decay, decay)))
                a, b = scanned(decay, m * inject * conv, d == 1)
                cum[d, :, lanes] = a
                loc[d, :, lanes] = b
                edge = rows - 1 if d == 0 else 0
                ends[layer, s, 2 * d : 2 * d + 1, lanes] = a[edge : edge + 1]
                ends[layer, s, 2 * d + 1 : 2 * d + 2, lanes] = b[edge : edge + 1]
            serve(1)

        def e_copy(source, d, to):
            return remote(
                ends.at[layer, source], ends.at[layer, source],
                e_send.at[layer, d], e_recv.at[layer, source], "sp", to,
            )

        for d in range(1, n_sp):
            e_copy(s, d, lax.rem(s + d, n_sp)).start()
        serve_until(wo)
        for d in range(1, n_sp):
            source = lax.rem(s + d, n_sp)
            e_copy(source, d, source).wait_recv()
        forward = jnp.zeros((1, channels), jnp.float32)
        backward = forward
        for step in range(n_sp - 1):
            forward = jnp.where(
                step < s, ends[layer, step, 0:1] * forward + ends[layer, step, 1:2], forward
            )
            back = n_sp - 1 - step
            backward = jnp.where(
                back > s, ends[layer, back, 2:3] * backward + ends[layer, back, 3:4], backward
            )
        state = loc[0] + cum[0] * forward + loc[1] + cum[1] * backward
        gated[...] = (state * y_act[...]).astype(jnp.bfloat16)

        def r_copy(source, slot, to):
            return remote(
                parts.at[layer, to], sums.at[layer, source],
                r_send.at[layer, slot], r_recv.at[layer, source], "tp", to,
            )

        landed(wo)
        for c in range(n_sp):
            partial = jnp.dot(gated[...], g_out[layer, c], preferred_element_type=jnp.float32)
            partial = partial.astype(jnp.bfloat16)
            for q in range(cs // piece):
                at = c * cs + q * piece
                j = at // ds
                parts[layer, j, :, at % ds : at % ds + piece] = partial[
                    :, q * piece : (q + 1) * piece
                ]
                if (at + piece) % ds == 0:
                    @pl.when(j != t)
                    def _():
                        r_copy(t, j, j).start()

        if layer == 0:
            serve(n_sp - 1)
        new = full[layer, t].astype(jnp.float32) + parts[layer, t].astype(jnp.float32)
        for d in tp_order:
            source = lax.rem(t + d, n_tp)
            r_copy(source, source, source).wait_recv()
            new = new + sums[layer, source].astype(jnp.float32)
        new = new.astype(jnp.bfloat16)
        if layer + 1 < layers:
            full[layer + 1, t] = new
            send_features(layer + 1, full.at[layer + 1, t])
        else:
            out[...] = new

    for w in range(weights):
        @pl.when(s < n_sp - 1)
        def _():
            z_copy(w, s, mine(w), s + 1, s).wait_send()

        @pl.when(s > 0)
        def _():
            z_copy(w, s, mine(w), s - 1, n_sp).wait_send()

        for c in range(n_sp):
            @pl.when(((c < s) & (s < n_sp - 1)) | ((c > s) & (s > 0)))
            def _():
                z_copy(w, c, hold(w, c), lax.rem(s + 1, n_sp), c).wait_send()

            if has_y(w):
                @pl.when(c != s)
                def _():
                    y_copy(w, c, g).wait_send()

    for layer in range(layers):
        for d in tp_order:
            f_copy(layer, full.at[layer, t], t, d, lax.rem(t + d, n_tp)).wait_send()
        for j in range(n_tp):
            @pl.when(j != t)
            def _():
                remote(
                    parts.at[layer, j], sums.at[layer, t],
                    r_send.at[layer, j], r_recv.at[layer, t], "tp", j,
                ).wait_send()

        for d in range(1, n_sp):
            remote(
                ends.at[layer, s], ends.at[layer, s],
                e_send.at[layer, d], e_recv.at[layer, s], "sp", lax.rem(s + d, n_sp),
            ).wait_send()

        @pl.when(s < n_sp - 1)
        def _():
            remote(
                xpad.at[layer, pl.ds(rows, HALO)], xpad.at[layer, pl.ds(0, HALO)],
                h_send.at[layer, 0], h_recv.at[layer, 0], "sp", lax.rem(s + 1, n_sp),
            ).wait_send()

        @pl.when(s > 0)
        def _():
            remote(
                xpad.at[layer, pl.ds(HALO, HALO)], xpad.at[layer, pl.ds(HALO + rows, HALO)],
                h_send.at[layer, 1], h_recv.at[layer, 1], "sp", lax.rem(s + n_sp - 1, n_sp),
            ).wait_send()


def solution(mesh):
    n_grp, n_sp, n_tp = mesh.shape["grp"], mesh.shape["sp"], mesh.shape["tp"]

    def local(stream, gain, conv_w, gate_w, out_w, taps, blocks, logit, boost):
        layers, cs, channels = conv_w.shape
        rows, ds = stream.shape
        rate = (-RECURRENT_WIDTH * jax.nn.softplus(-logit)).reshape(-1, channels)
        boost = boost.reshape(-1, rows).T
        bf, f32, dma = jnp.bfloat16, jnp.float32, pltpu.SemaphoreType.DMA
        vmem = pltpu.VMEM
        return pl.pallas_call(
            functools.partial(kernel, n_grp, n_sp, n_tp),
            out_shape=jax.ShapeDtypeStruct((rows, ds), bf),
            in_specs=[pl.BlockSpec(memory_space=vmem)] * 9,
            out_specs=pl.BlockSpec(memory_space=vmem),
            scratch_shapes=[
                vmem((layers, n_tp, rows, ds), bf),
                vmem((n_sp, rows, cs), bf),
                vmem((2 * layers, n_sp, cs, channels), bf),
                vmem((layers, n_sp, channels, cs), bf),
                vmem((layers, rows + 2 * HALO, channels), f32),
                vmem((rows, channels), f32),
                vmem((2, rows, channels), f32),
                vmem((2, rows, channels), f32),
                vmem((layers, n_sp, 8, channels), f32),
                vmem((rows, channels), bf),
                vmem((layers, n_tp, rows, ds), bf),
                vmem((layers, n_tp, rows, ds), bf),
                dma((3 * layers, n_sp + 1)),
                dma((3 * layers, n_sp)),
                dma((3 * layers, n_sp)),
                dma((3 * layers, n_sp)),
                dma((layers, n_tp)),
                dma((layers, n_tp)),
                dma((layers, n_tp)),
                dma((layers, n_tp)),
                dma((layers, 2)),
                dma((layers, 2)),
                dma((layers, n_sp)),
                dma((layers, n_sp)),
            ],
            compiler_params=pltpu.CompilerParams(
                collective_id=0, has_side_effects=True, vmem_limit_bytes=60 * 1024 * 1024
            ),
        )(stream, gain, conv_w, gate_w, out_w, taps, blocks, rate, boost)

    return jax.shard_map(
        local,
        mesh=mesh,
        in_specs=(
            P(("grp", "sp"), "tp"),
            P(),
            P(None, "sp", "tp"),
            P(None, "sp", "tp"),
            P(None, "tp", "sp"),
            P(None, None, "tp"),
            P(None, None, None, "tp", None, None),
            P(None, None, "tp"),
            P(None, None, ("grp", "sp")),
        ),
        out_specs=P(("grp", "sp"), "tp"),
        check_vma=False,
    )
```

profile of v0, /device:TPU:0, one launch (start us, length us, event | category | flops | bytes accessed | tf_op | source)
XLA Modules:
  0.0 138.1 jit_solution(18310073384874064984)
XLA Ops:
  0.0 0.0 copy-start
  0.0 0.7 reshape.7
  0.7 0.0 copy-done
  0.7 0.6 reshape.6.rate
  1.4 0.8 copy.11
  2.2 134.2 %shard_map.91 = bf16[256,512]{1,0:T(8,128)(2,1)} custom-call(bf16[256,512]{1,0:T(8,128)(2,1)} %stream.1, f32[2,2048]{1,0:T(2,128)} %gain.1, bf16[2,512,384]{2,1,0:T(8,128)(2,1)} %conv_w.1, bf16[2,512,384]{2,1,0:T(8,128)(2,1)} %gate_w.1, bf16[2,384,512]{2,1,0:T(8,128)(2,1)} %out_w.1, f32[2,4,384]{2,1,0:T(4,128)} %taps.1, ...), custom_call_target="tpu_custom_call" | custom-call | tf_op jit(solution)/shard_map/pallas_call | solution.py:411
  136.4 1.7 %copy.13 = bf16[256,512]{1,0:T(8,128)(2,1)} copy(bf16[256,512]{1,0:T(8,128)(2,1)} %shard_map.91) | data formatting | bytes 524288
  (1 shorter events, 0.0 us)
Async XLA Ops:
  0.0 0.7 copy-start
where the time goes:
time: 138 us
  Pallas kernels  134 us (97%)
  local copies, waits for them, and re-layouts  3.8 us (3%)
    pallas_call x1, Pallas kernels, local(): pl.pallas_call(functools.partial(kernel, n_grp, n_sp, n_tp), out_shape=ja...  134 us

commit v1 on v0

--- a/solution.py
+++ b/solution.py
@@ -398,16 +398,593 @@
             ).wait_send()
 
 
+def folded_kernel(
+    n_grp, n_sp, n_tp,
+    stream, gain, conv_w, gate_w, out_w, taps, blocks, rate, boost,
+    out,
+    full, normed, g_in, g_out, xpad, p_out, p_in, y_act, cum, loc, ends, gated,
+    a_out, a_in, own, b_out, b_in,
+    own_send, mid_send, in_send, out_send, y_send, w_recv,
+    s_send, s_recv, x_send, x_recv, c_send, c_recv, p_send, p_recv,
+    h_send, h_recv, e_send, e_recv, a_send, a_recv, b_send, b_recv,
+):
+    g, s, t = lax.axis_index("grp"), lax.axis_index("sp"), lax.axis_index("tp")
+    layers = conv_w.shape[0]
+    rows, ds = stream.shape
+    cs, channels = conv_w.shape[1], conv_w.shape[2]
+    width = blocks.shape[-1]
+    groups = channels // width
+    weights = 3 * layers
+    last = n_sp - 1
+    half = s // 2
+    end, mid = last * half, 1 + half
+    far_mid, far_end = last - mid, last - end
+    is_end = s == end
+    is_mid = s == mid
+    near = end + mid - s
+    chip, core = t // 2, t % 2
+    across, partner = lax.rem(t + 2, n_tp), t + 1 - 2 * core
+    guest = layers
+    slots = (near, far_mid, far_end)
+
+    def remote(src, dst, send, recv, axis, place):
+        return pltpu.make_async_remote_copy(
+            src_ref=src, dst_ref=dst, send_sem=send, recv_sem=recv,
+            device_id={axis: place}, device_id_type=MESH,
+        )
+
+    started = []
+
+    def launch(copy, cond=None):
+        started.append((copy, cond))
+        if cond is None:
+            copy.start()
+        else:
+            @pl.when(cond)
+            def _():
+                copy.start()
+
+    barrier = pltpu.get_barrier_semaphore()
+    total = 0
+    for axis, me, count in (("sp", s, n_sp), ("tp", t, n_tp), ("grp", g, n_grp)):
+        for d in range(1, count):
+            pl.semaphore_signal(
+                barrier, inc=1, device_id={axis: lax.rem(me + d, count)}, device_id_type=MESH
+            )
+            total += 1
+    pl.semaphore_wait(barrier, total)
+
+    def mine(w):
+        return (conv_w, gate_w, out_w)[w % 3].at[w // 3]
+
+    def place(w, slot, chunk):
+        return g_out.at[w // 3, chunk] if w % 3 == 2 else g_in.at[w // 3 * 2 + w % 3, slot]
+
+    def quarter(w, i):
+        size = (channels if w % 3 == 2 else cs) // 4
+        index = 2 * g + i if i < 2 else 2 * (1 - g) + i - 2
+        return pl.ds(pl.multiple_of(index * size, TILE), size)
+
+    def whole(w):
+        return w >= 1
+
+    def own_to_near(w, i):
+        q = quarter(w, i)
+        return remote(
+            mine(w).at[q], place(w, 0, s).at[q],
+            own_send.at[w, i], w_recv.at[w, 0, i], "sp", near,
+        )
+
+    def own_to_mid(w, i):
+        q = quarter(w, i)
+        return remote(
+            mine(w).at[q], place(w, 1, s).at[q],
+            mid_send.at[w, i], w_recv.at[w, 1, i], "sp", far_mid,
+        )
+
+    def pass_in(w, i):
+        q = quarter(w, i)
+        return remote(
+            place(w, 0, near).at[q], place(w, 2, near).at[q],
+            in_send.at[w, i], w_recv.at[w, 2, i], "sp", far_mid,
+        )
+
+    def pass_out(w, slot, i):
+        here = place(w, slot, slots[slot]).at[quarter(w, i)]
+        return remote(
+            here, here, out_send.at[w, slot - 1, i], w_recv.at[w, slot, i], "sp", near
+        )
+
+    def share(w, slot, i):
+        here = place(w, slot, slots[slot]).at[quarter(w, i)]
+        return remote(
+            here, here, y_send.at[w, slot, i], w_recv.at[w, slot, 2 + i], "grp", 1 - g
+        )
+
+    def arrived(w, slot, i):
+        here = place(w, slot, slots[slot]).at[quarter(w, i)]
+        remote(
+            here, here, y_send.at[w, slot, 0], w_recv.at[w, slot, i], "grp", 1 - g
+        ).wait_recv()
+
+    outgoing = [(w, i) for w in range(weights) for i in range(4 if whole(w) else 2)]
+
+    def send_outgoing(count):
+        for _ in range(min(count, len(outgoing))):
+            launch(own_to_near(*outgoing.pop(0)), is_end)
+
+    early = 2 * (weights - 2)
+
+    def tick(n):
+        w, i = n // 4, n % 4
+        slot, p = 1 + i // 2, i % 2
+
+        if n < early:
+            launch(own_to_near(2 + n // 2, n % 2), is_mid)
+
+        if i < 2 and w + 2 < weights:
+            launch(own_to_mid(w + 2, i), is_mid)
+
+        @pl.when(is_mid)
+        def _():
+            arrived(w, slot, p)
+
+        launch(share(w, slot, p), is_mid)
+        if w >= 2:
+            launch(pass_out(w, slot, p), is_mid)
+        if i < 2:
+            @pl.when(is_mid)
+            def _():
+                arrived(w, 0, p)
+
+            launch(pass_in(w, p), is_mid)
+            if not whole(w):
+                launch(share(w, 0, p), is_mid)
+
+        send_outgoing(1)
+        if n < early:
+            @pl.when(is_end)
+            def _():
+                arrived(2 + n // 2, 0, n % 2)
+
+            launch(share(2 + n // 2, 0, n % 2), is_end)
+        if w >= 2:
+            @pl.when(is_end)
+            def _():
+                arrived(w, slot, p)
+
+            launch(share(w, slot, p), is_end)
+
+    ticks = list(range(4 * weights))
+
+    def serve_to(n):
+        while ticks and ticks[0] < n:
+            tick(ticks.pop(0))
+
+    def landed(w):
+        serve_to(4 * w + 4)
+
+        def wait_all():
+            for slot in range(3):
+                for i in (2, 3):
+                    arrived(w, slot, i)
+
+        if w < 2:
+            pl.when(is_mid)(wait_all)
+        else:
+            wait_all()
+
+    pieces = 2
+    part = rows // pieces
+
+    def strip(p):
+        return pl.ds(p * part, part)
+
+    def guest_copy(p):
+        return remote(
+            stream.at[strip(p)], full.at[guest, t, strip(p)],
+            s_send.at[p], s_recv.at[p], "sp", mid,
+        )
+
+    def across_copy(k, p, src):
+        return remote(
+            src.at[strip(p)], full.at[k, t, strip(p)],
+            x_send.at[k, p], x_recv.at[k, p], "tp", across,
+        )
+
+    def core_copy(k, p, src):
+        return remote(
+            src.at[strip(p)], full.at[k, t, strip(p)],
+            c_send.at[k, p, 0], c_recv.at[k, p, 0], "tp", partner,
+        )
+
+    def hand_copy(k, p):
+        here = full.at[k, across, strip(p)]
+        return remote(here, here, c_send.at[k, p, 1], c_recv.at[k, p, 1], "tp", partner)
+
+    def spread(k, p, src, cond=None):
+        launch(across_copy(k, p, src), cond)
+        launch(core_copy(k, p, src), cond)
+
+    def hand_on(k, p, cond=None):
+        copy = across_copy(k, p, full.at[k, t])
+        if cond is None:
+            copy.wait_recv()
+        else:
+            @pl.when(cond)
+            def _():
+                copy.wait_recv()
+
+        launch(hand_copy(k, p), cond)
+
+    def gathered(k):
+        for p in range(pieces):
+            core_copy(k, p, full.at[k, t]).wait_recv()
+            hand_copy(k, p).wait_recv()
+
+    def normalise(layer, k, slot):
+        square = jnp.zeros((rows, 1), jnp.float32)
+        for j in range(n_tp):
+            x = full[k, j].astype(jnp.float32)
+            square += jnp.sum(x * x, axis=-1, keepdims=True)
+        inverse = lax.rsqrt(square / (n_tp * ds) + EPS)
+        for j in range(n_tp):
+            x = full[k, j].astype(jnp.float32)
+            x = x * inverse * gain[layer : layer + 1, j * ds : (j + 1) * ds]
+            normed[slot, j] = x.astype(jnp.bfloat16)
+
+    def project(w, slot):
+        acc = jnp.dot(
+            normed[slot, s], mine(w)[...], preferred_element_type=jnp.float32
+        )
+        for k in range(3):
+            acc += jnp.dot(
+                normed[slot, slots[k]], g_in[w // 3 * 2 + w % 3, k],
+                preferred_element_type=jnp.float32,
+            )
+        return acc.astype(jnp.bfloat16)
+
+    def p_copy(j, n):
+        return remote(
+            p_out.at[j, n], p_in.at[j, n], p_send.at[j, n], p_recv.at[j, n], "sp", near
+        )
+
+    def halo_right(layer):
+        return remote(
+            xpad.at[layer, pl.ds(rows, HALO)], xpad.at[layer, pl.ds(0, HALO)],
+            h_send.at[layer, 0], h_recv.at[layer, 0], "sp", lax.rem(s + 1, n_sp),
+        )
+
+    def halo_left(layer):
+        return remote(
+            xpad.at[layer, pl.ds(HALO, HALO)], xpad.at[layer, pl.ds(HALO + rows, HALO)],
+            h_send.at[layer, 1], h_recv.at[layer, 1], "sp", lax.rem(s + n_sp - 1, n_sp),
+        )
+
+    row = lax.broadcasted_iota(jnp.int32, (rows, 1), 0)
+    diagonal = lax.broadcasted_iota(jnp.int32, (rows, rows), 0) == lax.broadcasted_iota(
+        jnp.int32, (rows, rows), 1
+    )
+
+    def recurrences(layer, n):
+        lanes = slice(n * width, (n + 1) * width)
+        conv = None
+        for k in range(taps.shape[1]):
+            term = taps[layer, k : k + 1, lanes] * xpad[
+                layer, HALO - 1 + k : HALO - 1 + k + rows, lanes
+            ]
+            conv = term if conv is None else conv + term
+        conv_half = conv.astype(jnp.bfloat16)
+        conv = conv_half.astype(jnp.float32)
+        for d in range(2):
+            recur = jax.nn.sigmoid(
+                jnp.dot(conv_half, blocks[layer, d, 0, n], preferred_element_type=jnp.float32)
+            )
+            inject = jax.nn.sigmoid(
+                jnp.dot(conv_half, blocks[layer, d, 1, n], preferred_element_type=jnp.float32)
+            )
+            lift = jnp.sum(
+                jnp.where(diagonal, boost[layer, d : d + 1], 0.0), axis=1, keepdims=True
+            )
+            log_decay = rate[layer, d : d + 1, lanes] * recur + lift
+            decay = jnp.exp(log_decay)
+            first = (row == 0) & (s == 0) if d == 0 else (row == rows - 1) & (s == last)
+            m = jnp.where(first, 1.0, jnp.sqrt(one_minus_square(log_decay, decay)))
+            a, b = scanned(decay, m * inject * conv, d == 1)
+            cum[d, :, lanes] = a
+            loc[d, :, lanes] = b
+            edge = rows - 1 if d == 0 else 0
+            ends[layer, s, 2 * d : 2 * d + 1, lanes] = a[edge : edge + 1]
+            ends[layer, s, 2 * d + 1 : 2 * d + 2, lanes] = b[edge : edge + 1]
+
+    def e_copy(layer, source, d, to):
+        return remote(
+            ends.at[layer, source], ends.at[layer, source],
+            e_send.at[layer, d], e_recv.at[layer, source], "sp", to,
+        )
+
+    def send_ends(layer):
+        for d in range(1, n_sp):
+            launch(e_copy(layer, s, d, lax.rem(s + d, n_sp)))
+
+    def states(layer):
+        for d in range(1, n_sp):
+            source = lax.rem(s + d, n_sp)
+            e_copy(layer, source, d, source).wait_recv()
+        forward = jnp.zeros((1, channels), jnp.float32)
+        backward = forward
+        for step in range(n_sp - 1):
+            forward = jnp.where(
+                step < s, ends[layer, step, 0:1] * forward + ends[layer, step, 1:2], forward
+            )
+            back = n_sp - 1 - step
+            backward = jnp.where(
+                back > s, ends[layer, back, 2:3] * backward + ends[layer, back, 3:4], backward
+            )
+        state = loc[0] + cum[0] * forward + loc[1] + cum[1] * backward
+        gated[...] = (state * y_act[...]).astype(jnp.bfloat16)
+
+    def a_copy(layer, k):
+        return remote(
+            a_out.at[layer, k], a_in.at[layer, k],
+            a_send.at[layer, k], a_recv.at[layer, k], "tp", partner,
+        )
+
+    def b_copy(layer, p):
+        return remote(
+            b_out.at[layer, strip(p)], b_in.at[layer, strip(p)],
+            b_send.at[layer, p], b_recv.at[layer, p], "tp", across,
+        )
+
+    def branch(layer, j):
+        return jnp.dot(gated[...], g_out[layer, j], preferred_element_type=jnp.float32)
+
+    def project_out(layer):
+        chips = (1 - chip, chip)
+        for k in range(2):
+            a_out[layer, k] = branch(layer, 2 * chips[k] + 1 - core).astype(jnp.bfloat16)
+            launch(a_copy(layer, k))
+        for k in range(2):
+            own[k] = branch(layer, 2 * chips[k] + core)
+        a_copy(layer, 0).wait_recv()
+        for p in range(pieces):
+            here = slice(p * part, (p + 1) * part)
+            b_out[layer, here] = (
+                own[0, here] + a_in[layer, 0, here].astype(jnp.float32)
+            ).astype(jnp.bfloat16)
+            launch(b_copy(layer, p))
+        a_copy(layer, 1).wait_recv()
+        own[1] += a_in[layer, 1].astype(jnp.float32)
+
+    def finish(layer, p, old):
+        here = slice(p * part, (p + 1) * part)
+        b_copy(layer, p).wait_recv()
+        new = old[here].astype(jnp.float32) + own[1, here]
+        return (new + b_in[layer, here].astype(jnp.float32)).astype(jnp.bfloat16)
+
+    send_outgoing(2)
+    for p in range(pieces):
+        launch(guest_copy(p), is_end)
+        spread(0, p, stream, is_mid)
+    send_outgoing(1)
+    for w in range(min(2, weights)):
+        for i in range(2):
+            launch(own_to_mid(w, i), is_mid)
+    full[0, t] = stream[...]
+    for layer in range(layers):
+        g_out[layer, s] = out_w[layer]
+
+    serve_to(2)
+    for p in range(pieces):
+        hand_on(0, p, is_mid)
+    for p in range(pieces):
+        serve_to(3 + p)
+
+        @pl.when(is_mid)
+        def _():
+            guest_copy(p).wait_recv()
+
+        spread(guest, p, full.at[guest, t], is_mid)
+
+    @pl.when(is_mid)
+    def _():
+        gathered(0)
+        normalise(0, 0, 0)
+
+    serve_to(5)
+    landed(0)
+
+    @pl.when(is_mid)
+    def _():
+        xpad[0, HALO : HALO + rows] = project(0, 0).astype(jnp.float32)
+
+    launch(halo_right(0), is_mid)
+    launch(halo_left(0), is_mid)
+    serve_to(6)
+    for p in range(pieces):
+        hand_on(guest, p, is_mid)
+
+    @pl.when(is_mid)
+    def _():
+        gathered(guest)
+        normalise(0, guest, 1)
+        x = project(0, 1)
+        for n in range(groups):
+            p_out[0, n] = x[:, n * width : (n + 1) * width]
+
+        @pl.when(half == 0)
+        def _():
+            xpad[0, 0:HALO] = x[rows - HALO :].astype(jnp.float32)
+
+        @pl.when(half == 1)
+        def _():
+            xpad[0, HALO + rows : 2 * HALO + rows] = x[:HALO].astype(jnp.float32)
+
+    for n in range(groups):
+        launch(p_copy(0, n), is_mid)
+    serve_to(8)
+
+    @pl.when(is_end)
+    def _():
+        for n in range(groups):
+            p_copy(0, n).wait_recv()
+            xpad[0, HALO : HALO + rows, n * width : (n + 1) * width] = p_in[0, n].astype(
+                jnp.float32
+            )
+
+    for layer in range(layers):
+        wx, wy, wo = 3 * layer, 3 * layer + 1, 3 * layer + 2
+        if layer > 0:
+            for p in range(pieces):
+                hand_on(layer, p)
+            gathered(layer)
+            normalise(layer, layer, 0)
+            landed(wx)
+            xpad[layer, HALO : HALO + rows] = project(wx, 0).astype(jnp.float32)
+            launch(halo_right(layer), s < last)
+            launch(halo_left(layer), s > 0)
+
+        @pl.when((s > 0) if layer > 0 else (s >= 2))
+        def _():
+            halo_right(layer).wait_recv()
+
+        @pl.when(s == 0)
+        def _():
+            xpad[layer, 0:HALO] = jnp.zeros((HALO, channels), jnp.float32)
+
+        @pl.when((s < last) if layer > 0 else (s < 2))
+        def _():
+            halo_left(layer).wait_recv()
+
+        @pl.when(s == last)
+        def _():
+            xpad[layer, HALO + rows : 2 * HALO + rows] = jnp.zeros((HALO, channels), jnp.float32)
+
+        for n in range(groups):
+            recurrences(layer, n)
+            serve_to(4 * wy + 2 + n)
+        send_ends(layer)
+        landed(wy)
+        if layer == 0:
+            @pl.when(is_mid)
+            def _():
+                y = project(wy, 1)
+                for n in range(groups):
+                    p_out[1, n] = y[:, n * width : (n + 1) * width]
+
+            for n in range(groups):
+                launch(p_copy(1, n), is_mid)
+
+            @pl.when(is_mid)
+            def _():
+                y_act[...] = jax.nn.gelu(project(wy, 0).astype(jnp.float32))
+
+            serve_to(4 * wo + 2)
+
+            @pl.when(is_end)
+            def _():
+                for n in range(groups):
+                    p_copy(1, n).wait_recv()
+                    y_act[:, n * width : (n + 1) * width] = jax.nn.gelu(
+                        p_in[1, n].astype(jnp.float32)
+                    )
+        else:
+            y_act[...] = jax.nn.gelu(project(wy, 0).astype(jnp.float32))
+        states(layer)
+        landed(wo)
+        project_out(layer)
+        if layer + 1 < layers:
+            serve_to(4 * wo + 6)
+            for p in range(pieces):
+                full[layer + 1, t, p * part : (p + 1) * part] = finish(
+                    layer, p, stream if layer == 0 else full.at[layer, t]
+                )
+                spread(layer + 1, p, full.at[layer + 1, t])
+            serve_to(4 * wo + 8)
+        else:
+            for p in range(pieces):
+                out[p * part : (p + 1) * part] = finish(layer, p, full.at[layer, t])
+
+    for copy, cond in started:
+        if cond is None:
+            copy.wait_send()
+        else:
+            @pl.when(cond)
+            def _():
+                copy.wait_send()
+
+
+def folds(n_grp, n_sp, n_tp, layers, rows, ds, cs, channels):
+    return (
+        n_grp == 2 and n_sp == 4 and n_tp == n_sp and cs == ds
+        and rows % (2 * TILE) == 0 and cs % (4 * TILE) == 0 and channels % (4 * TILE) == 0
+    )
+
+
 def solution(mesh):
     n_grp, n_sp, n_tp = mesh.shape["grp"], mesh.shape["sp"], mesh.shape["tp"]
 
     def local(stream, gain, conv_w, gate_w, out_w, taps, blocks, logit, boost):
         layers, cs, channels = conv_w.shape
         rows, ds = stream.shape
-        rate = (-RECURRENT_WIDTH * jax.nn.softplus(-logit)).reshape(-1, channels)
-        boost = boost.reshape(-1, rows).T
+        width = blocks.shape[-1]
         bf, f32, dma = jnp.bfloat16, jnp.float32, pltpu.SemaphoreType.DMA
         vmem = pltpu.VMEM
+        rate = -RECURRENT_WIDTH * jax.nn.softplus(-logit)
+        if folds(n_grp, n_sp, n_tp, layers, rows, ds, cs, channels):
+            weights, groups = 3 * layers, channels // width
+            return pl.pallas_call(
+                functools.partial(folded_kernel, n_grp, n_sp, n_tp),
+                out_shape=jax.ShapeDtypeStruct((rows, ds), bf),
+                in_specs=[pl.BlockSpec(memory_space=vmem)] * 9,
+                out_specs=pl.BlockSpec(memory_space=vmem),
+                scratch_shapes=[
+                    vmem((layers + 1, n_tp, rows, ds), bf),
+                    vmem((2, n_sp, rows, cs), bf),
+                    vmem((2 * layers, 3, cs, channels), bf),
+                    vmem((layers, n_sp, channels, cs), bf),
+                    vmem((layers, rows + 2 * HALO, channels), f32),
+                    vmem((2, groups, rows, width), bf),
+                    vmem((2, groups, rows, width), bf),
+                    vmem((rows, channels), f32),
+                    vmem((2, rows, channels), f32),
+                    vmem((2, rows, channels), f32),
+                    vmem((layers, n_sp, 8, channels), f32),
+                    vmem((rows, channels), bf),
+                    vmem((layers, 2, rows, ds), bf),
+                    vmem((layers, 2, rows, ds), bf),
+                    vmem((2, rows, ds), f32),
+                    vmem((layers, rows, ds), bf),
+                    vmem((layers, rows, ds), bf),
+                    dma((weights, 4)),
+                    dma((weights, 2)),
+                    dma((weights, 2)),
+                    dma((weights, 2, 2)),
+                    dma((weights, 3, 2)),
+                    dma((weights, 3, 4)),
+                    dma((2,)),
+                    dma((2,)),
+                    dma((layers + 1, 2)),
+                    dma((layers + 1, 2)),
+                    dma((layers + 1, 2, 2)),
+                    dma((layers + 1, 2, 2)),
+                    dma((2, groups)),
+                    dma((2, groups)),
+                    dma((layers, 2)),
+                    dma((layers, 2)),
+                    dma((layers, n_sp)),
+                    dma((layers, n_sp)),
+                    dma((layers, 2)),
+                    dma((layers, 2)),
+                    dma((layers, 2)),
+                    dma((layers, 2)),
+                ],
+                compiler_params=pltpu.CompilerParams(
+                    collective_id=0, has_side_effects=True, vmem_limit_bytes=60 * 1024 * 1024
+                ),
+            )(stream, gain, conv_w, gate_w, out_w, taps, blocks, rate, boost)
+        rate = rate.reshape(-1, channels)
+        boost = boost.reshape(-1, rows).T
         return pl.pallas_call(
             functools.partial(kernel, n_grp, n_sp, n_tp),
             out_shape=jax.ShapeDtypeStruct((rows, ds), bf),

time: 138 us -> 123 us (0.89)
  Pallas kernels: 134 us -> 120 us
  local copies, waits for them, and re-layouts: 3.8 us -> 1.67 us
    pallas_call x1, Pallas kernels: 134 us -> 120 us  [local(): pl.pallas_call(functools.partial(folded_kernel, n_grp, n_sp, n_tp), out_s...]
    reshape x3 -> x0, local copies, waits for them, and re-layouts: 2.12 us -> none  [the longest x2 1.51 us: local(): boost = boost.reshape(-1, rows).T]
where the time goes in v1:
time: 123 us
  Pallas kernels  120 us (98%)
  local copies, waits for them, and re-layouts  1.67 us (1%)
  other arithmetic  1.31 us (1%)
    pallas_call x1, Pallas kernels, local(): pl.pallas_call(functools.partial(folded_kernel, n_grp, n_sp, n_tp), out_s...  120 us

profile of v1, /device:TPU:0, one launch (start us, length us, event | category | flops | bytes accessed | tf_op | source)
XLA Modules:
  0.0 122.9 jit_solution(17595240418258388015)
XLA Ops:
  0.0 1.3 %fusion.rate = f32[2,2,384]{2,1,0:T(2,128)} fusion(f32[2,2,384]{2,1,0:T(2,128)} %param.16), kind=kLoop, calls=%fused_computation.1 | loop fusion | flops 12288 | bytes 12288 | tf_op jit(solution)/shard_map/mul | solution.py:933
  1.3 119.9 %shard_map.91 = bf16[256,512]{1,0:T(8,128)(2,1)} custom-call(bf16[256,512]{1,0:T(8,128)(2,1)} %stream.1, f32[2,2048]{1,0:T(2,128)} %gain.1, bf16[2,512,384]{2,1,0:T(8,128)(2,1)} %conv_w.1, bf16[2,512,384]{2,1,0:T(8,128)(2,1)} %gate_w.1, bf16[2,384,512]{2,1,0:T(8,128)(2,1)} %out_w.1, f32[2,4,384]{2,1,0:T(4,128)} %taps.1, ...), custom_call_target="tpu_custom_call" | custom-call | tf_op jit(solution)/shard_map/pallas_call | solution.py:936
  121.2 1.7 %copy.11 = bf16[256,512]{1,0:T(8,128)(2,1)} copy(bf16[256,512]{1,0:T(8,128)(2,1)} %shard_map.91) | data formatting | bytes 524288

commit v2 on v1

--- a/solution.py
+++ b/solution.py
@@ -11,6 +11,9 @@
 RECURRENT_WIDTH = 8.0
 TILE = 16
 HALO = 8
+LAG = 0
+END_LAG = 0
+PIECES = 4
 MESH = pl.DeviceIdType.MESH
 
 
@@ -513,17 +516,17 @@
         for _ in range(min(count, len(outgoing))):
             launch(own_to_near(*outgoing.pop(0)), is_end)
 
+    inward = [(w, i) for w in range(weights) for i in range(2)]
+
+    def send_inward(count):
+        for _ in range(min(count, len(inward))):
+            launch(own_to_mid(*inward.pop(0)), is_mid)
+
     early = 2 * (weights - 2)
 
-    def tick(n):
+    def mid_tick(n):
         w, i = n // 4, n % 4
         slot, p = 1 + i // 2, i % 2
-
-        if n < early:
-            launch(own_to_near(2 + n // 2, n % 2), is_mid)
-
-        if i < 2 and w + 2 < weights:
-            launch(own_to_mid(w + 2, i), is_mid)
 
         @pl.when(is_mid)
         def _():
@@ -540,8 +543,14 @@
             launch(pass_in(w, p), is_mid)
             if not whole(w):
                 launch(share(w, 0, p), is_mid)
-
-        send_outgoing(1)
+            if i == 1:
+                send_inward(2)
+
+    def end_tick(n):
+        w, i = n // 4, n % 4
+        slot, p = 1 + i // 2, i % 2
+        if n >= 2:
+            send_outgoing(1)
         if n < early:
             @pl.when(is_end)
             def _():
@@ -555,14 +564,17 @@
 
             launch(share(w, slot, p), is_end)
 
-    ticks = list(range(4 * weights))
-
-    def serve_to(n):
-        while ticks and ticks[0] < n:
-            tick(ticks.pop(0))
+    mid_ticks = list(range(4 * weights))
+    end_ticks = list(range(4 * weights))
+
+    def serve(mid=0, end=0):
+        while mid_ticks and mid_ticks[0] < mid:
+            mid_tick(mid_ticks.pop(0))
+        while end_ticks and end_ticks[0] < end:
+            end_tick(end_ticks.pop(0))
 
     def landed(w):
-        serve_to(4 * w + 4)
+        serve(4 * w + 4 + LAG, 4 * w + 4 + END_LAG if w >= 2 else 0)
 
         def wait_all():
             for slot in range(3):
@@ -574,7 +586,7 @@
         else:
             wait_all()
 
-    pieces = 2
+    pieces = PIECES
     part = rows // pieces
 
     def strip(p):
@@ -766,48 +778,45 @@
     for p in range(pieces):
         launch(guest_copy(p), is_end)
         spread(0, p, stream, is_mid)
-    send_outgoing(1)
-    for w in range(min(2, weights)):
-        for i in range(2):
-            launch(own_to_mid(w, i), is_mid)
+    send_outgoing(0)
+    send_inward(2)
+    for n in range(early):
+        launch(own_to_near(2 + n // 2, n % 2), is_mid)
     full[0, t] = stream[...]
     for layer in range(layers):
         g_out[layer, s] = out_w[layer]
 
-    serve_to(2)
+    serve(2, 4)
     for p in range(pieces):
         hand_on(0, p, is_mid)
     for p in range(pieces):
-        serve_to(3 + p)
+        serve(2 + (2 * p + 1) // pieces)
 
         @pl.when(is_mid)
         def _():
             guest_copy(p).wait_recv()
 
         spread(guest, p, full.at[guest, t], is_mid)
+    serve(4)
 
     @pl.when(is_mid)
     def _():
         gathered(0)
         normalise(0, 0, 0)
 
-    serve_to(5)
-    landed(0)
-
-    @pl.when(is_mid)
-    def _():
-        xpad[0, HALO : HALO + rows] = project(0, 0).astype(jnp.float32)
-
-    launch(halo_right(0), is_mid)
-    launch(halo_left(0), is_mid)
-    serve_to(6)
     for p in range(pieces):
         hand_on(guest, p, is_mid)
+    serve(6)
 
     @pl.when(is_mid)
     def _():
         gathered(guest)
         normalise(0, guest, 1)
+
+    landed(0)
+
+    @pl.when(is_mid)
+    def _():
         x = project(0, 1)
         for n in range(groups):
             p_out[0, n] = x[:, n * width : (n + 1) * width]
@@ -822,7 +831,15 @@
 
     for n in range(groups):
         launch(p_copy(0, n), is_mid)
-    serve_to(8)
+
+    @pl.when(is_mid)
+    def _():
+        xpad[0, HALO : HALO + rows] = project(0, 0).astype(jnp.float32)
+
+    launch(halo_right(0), is_mid)
+    launch(halo_left(0), is_mid)
+    serve(8, 8)
+    send_outgoing(4)
 
     @pl.when(is_end)
     def _():
@@ -837,12 +854,14 @@
         if layer > 0:
             for p in range(pieces):
                 hand_on(layer, p)
+                serve(4 * wx + 6 + 2 * p // pieces, 4 * wx + 6 + 2 * p // pieces)
             gathered(layer)
             normalise(layer, layer, 0)
             landed(wx)
             xpad[layer, HALO : HALO + rows] = project(wx, 0).astype(jnp.float32)
             launch(halo_right(layer), s < last)
             launch(halo_left(layer), s > 0)
+            serve(4 * wx + 11, 4 * wx + 9)
 
         @pl.when((s > 0) if layer > 0 else (s >= 2))
         def _():
@@ -862,8 +881,16 @@
 
         for n in range(groups):
             recurrences(layer, n)
-            serve_to(4 * wy + 2 + n)
+            if layer == 0:
+                serve(4 * wo + n)
+            else:
+                serve(4 * wx + 12)
         send_ends(layer)
+        if layer == 0:
+            send_outgoing(4)
+            serve(4 * wo + 4, 4 * wo + 2)
+        if layer == layers - 1:
+            serve(4 * weights, 24)
         landed(wy)
         if layer == 0:
             @pl.when(is_mid)
@@ -879,7 +906,7 @@
             def _():
                 y_act[...] = jax.nn.gelu(project(wy, 0).astype(jnp.float32))
 
-            serve_to(4 * wo + 2)
+            serve(4 * wo + 4, 4 * wo + 4)
 
             @pl.when(is_end)
             def _():
@@ -894,13 +921,12 @@
         landed(wo)
         project_out(layer)
         if layer + 1 < layers:
-            serve_to(4 * wo + 6)
             for p in range(pieces):
+                serve(4 * wo + 7 + 3 * p // pieces, 4 * wo + 6 + 4 * p // pieces)
                 full[layer + 1, t, p * part : (p + 1) * part] = finish(
                     layer, p, stream if layer == 0 else full.at[layer, t]
                 )
                 spread(layer + 1, p, full.at[layer + 1, t])
-            serve_to(4 * wo + 8)
         else:
             for p in range(pieces):
                 out[p * part : (p + 1) * part] = finish(layer, p, full.at[layer, t])
@@ -917,7 +943,7 @@
 def folds(n_grp, n_sp, n_tp, layers, rows, ds, cs, channels):
     return (
         n_grp == 2 and n_sp == 4 and n_tp == n_sp and cs == ds
-        and rows % (2 * TILE) == 0 and cs % (4 * TILE) == 0 and channels % (4 * TILE) == 0
+        and rows % (PIECES * TILE) == 0 and cs % (4 * TILE) == 0 and channels % (4 * TILE) == 0
     )
 
 
@@ -962,12 +988,12 @@
                     dma((weights, 2, 2)),
                     dma((weights, 3, 2)),
                     dma((weights, 3, 4)),
-                    dma((2,)),
-                    dma((2,)),
-                    dma((layers + 1, 2)),
-                    dma((layers + 1, 2)),
-                    dma((layers + 1, 2, 2)),
-                    dma((layers + 1, 2, 2)),
+                    dma((PIECES,)),
+                    dma((PIECES,)),
+                    dma((layers + 1, PIECES)),
+                    dma((layers + 1, PIECES)),
+                    dma((layers + 1, PIECES, 2)),
+                    dma((layers + 1, PIECES, 2)),
                     dma((2, groups)),
                     dma((2, groups)),
                     dma((layers, 2)),
@@ -976,8 +1002,8 @@
                     dma((layers, n_sp)),
                     dma((layers, 2)),
                     dma((layers, 2)),
-                    dma((layers, 2)),
-                    dma((layers, 2)),
+                    dma((layers, PIECES)),
+                    dma((layers, PIECES)),
                 ],
                 compiler_params=pltpu.CompilerParams(
                     collective_id=0, has_side_effects=True, vmem_limit_bytes=60 * 1024 * 1024

time: 123 us -> 94.8 us (0.77)
  Pallas kernels: 120 us -> 91.6 us
    pallas_call x1, Pallas kernels: 120 us -> 91.6 us  [local(): pl.pallas_call(functools.partial(folded_kernel, n_grp, n_sp, n_tp), out_s...]
where the time goes in v2:
time: 94.8 us; the launch traced here: 94.6 us
  Pallas kernels  91.6 us (97%)
  local copies, waits for them, and re-layouts  1.67 us (2%)
  other arithmetic  1.31 us (1%)
    pallas_call x1, Pallas kernels, local(): pl.pallas_call(functools.partial(folded_kernel, n_grp, n_sp, n_tp), out_s...  91.6 us

profile of v2, /device:TPU:0, one launch (start us, length us, event | category | flops | bytes accessed | tf_op | source)
XLA Modules:
  0.0 94.6 jit_solution(7447666068232607220)
XLA Ops:
  0.0 1.3 %fusion.rate = f32[2,2,384]{2,1,0:T(2,128)} fusion(f32[2,2,384]{2,1,0:T(2,128)} %param.16), kind=kLoop, calls=%fused_computation.1 | loop fusion | flops 12288 | bytes 12288 | tf_op jit(solution)/shard_map/mul | solution.py:959
  1.3 91.6 %shard_map.91 = bf16[256,512]{1,0:T(8,128)(2,1)} custom-call(bf16[256,512]{1,0:T(8,128)(2,1)} %stream.1, f32[2,2048]{1,0:T(2,128)} %gain.1, bf16[2,512,384]{2,1,0:T(8,128)(2,1)} %conv_w.1, bf16[2,512,384]{2,1,0:T(8,128)(2,1)} %gate_w.1, bf16[2,384,512]{2,1,0:T(8,128)(2,1)} %out_w.1, f32[2,4,384]{2,1,0:T(4,128)} %taps.1, ...), custom_call_target="tpu_custom_call" | custom-call | tf_op jit(solution)/shard_map/pallas_call | solution.py:962
  92.9 1.7 %copy.11 = bf16[256,512]{1,0:T(8,128)(2,1)} copy(bf16[256,512]{1,0:T(8,128)(2,1)} %shard_map.91) | data formatting | bytes 524288

commit v3 on v2

--- a/solution.py
+++ b/solution.py
@@ -401,19 +401,30 @@
             ).wait_send()
 
 
+def softplus(x):
+    u = jnp.exp(-jnp.abs(x))
+    w = u / (u + 2.0)
+    square = w * w
+    series = jnp.full_like(x, 1 / 19)
+    for k in range(17, 0, -2):
+        series = series * square + 1 / k
+    return jnp.maximum(x, 0.0) + 2.0 * w * series
+
+
 def folded_kernel(
     n_grp, n_sp, n_tp,
-    stream, gain, conv_w, gate_w, out_w, taps, blocks, rate, boost,
+    stream_in, gain_in, conv_in, gate_in, out_in, taps_in, blocks_in, logit_in, boost_in,
     out,
+    gain, conv_w, gate_w, taps, blocks, logit, boost, rate, load_sem,
     full, normed, g_in, g_out, xpad, p_out, p_in, y_act, cum, loc, ends, gated,
     a_out, a_in, own, b_out, b_in,
     own_send, mid_send, in_send, out_send, y_send, w_recv,
-    s_send, s_recv, x_send, x_recv, c_send, c_recv, p_send, p_recv,
+    guest_boost, g_send, g_recv, s_send, s_recv, x_send, x_recv, c_send, c_recv, p_send, p_recv,
     h_send, h_recv, e_send, e_recv, a_send, a_recv, b_send, b_recv,
 ):
     g, s, t = lax.axis_index("grp"), lax.axis_index("sp"), lax.axis_index("tp")
     layers = conv_w.shape[0]
-    rows, ds = stream.shape
+    rows, ds = stream_in.shape
     cs, channels = conv_w.shape[1], conv_w.shape[2]
     width = blocks.shape[-1]
     groups = channels // width
@@ -436,6 +447,19 @@
             device_id={axis: place}, device_id_type=MESH,
         )
 
+    stream = full.at[0, t]
+    loads = [
+        (stream_in, stream), (conv_in, conv_w), (gate_in, gate_w),
+        *((out_in.at[layer], g_out.at[layer, s]) for layer in range(layers)),
+        (logit_in, logit), (gain_in, gain), (taps_in, taps), (boost_in, boost),
+        (blocks_in, blocks),
+    ]
+    loads = [
+        pltpu.make_async_copy(src, dst, load_sem.at[i]) for i, (src, dst) in enumerate(loads)
+    ]
+    for load in loads:
+        load.start()
+
     started = []
 
     def launch(copy, cond=None):
@@ -456,9 +480,13 @@
             )
             total += 1
     pl.semaphore_wait(barrier, total)
+    for load in loads:
+        load.wait()
 
     def mine(w):
-        return (conv_w, gate_w, out_w)[w % 3].at[w // 3]
+        if w % 3 == 2:
+            return g_out.at[w // 3, s]
+        return (conv_w, gate_w)[w % 3].at[w // 3]
 
     def place(w, slot, chunk):
         return g_out.at[w // 3, chunk] if w % 3 == 2 else g_in.at[w // 3 * 2 + w % 3, slot]
@@ -656,9 +684,12 @@
             )
         return acc.astype(jnp.bfloat16)
 
-    def p_copy(j, n):
-        return remote(
-            p_out.at[j, n], p_in.at[j, n], p_send.at[j, n], p_recv.at[j, n], "sp", near
+    def p_copy(n):
+        return remote(p_out.at[n], p_in.at[n], p_send.at[n], p_recv.at[n], "sp", near)
+
+    def boost_copy():
+        return remote(
+            boost.at[0], guest_boost, g_send.at[0], g_recv.at[0], "sp", mid
         )
 
     def halo_right(layer):
@@ -678,12 +709,15 @@
         jnp.int32, (rows, rows), 1
     )
 
-    def recurrences(layer, n):
+    def recurrences(layer, n, k=0):
+        pad = guest if k else layer
+        block = end if k else s
+        raised = guest_boost if k else boost.at[layer]
         lanes = slice(n * width, (n + 1) * width)
         conv = None
-        for k in range(taps.shape[1]):
-            term = taps[layer, k : k + 1, lanes] * xpad[
-                layer, HALO - 1 + k : HALO - 1 + k + rows, lanes
+        for tap in range(taps.shape[1]):
+            term = taps[layer, tap : tap + 1, lanes] * xpad[
+                pad, HALO - 1 + tap : HALO - 1 + tap + rows, lanes
             ]
             conv = term if conv is None else conv + term
         conv_half = conv.astype(jnp.bfloat16)
@@ -696,18 +730,18 @@
                 jnp.dot(conv_half, blocks[layer, d, 1, n], preferred_element_type=jnp.float32)
             )
             lift = jnp.sum(
-                jnp.where(diagonal, boost[layer, d : d + 1], 0.0), axis=1, keepdims=True
+                jnp.where(diagonal, raised[d : d + 1], 0.0), axis=1, keepdims=True
             )
             log_decay = rate[layer, d : d + 1, lanes] * recur + lift
             decay = jnp.exp(log_decay)
-            first = (row == 0) & (s == 0) if d == 0 else (row == rows - 1) & (s == last)
+            first = (row == 0) & (block == 0) if d == 0 else (row == rows - 1) & (block == last)
             m = jnp.where(first, 1.0, jnp.sqrt(one_minus_square(log_decay, decay)))
             a, b = scanned(decay, m * inject * conv, d == 1)
-            cum[d, :, lanes] = a
-            loc[d, :, lanes] = b
+            cum[k, d, :, lanes] = a
+            loc[k, d, :, lanes] = b
             edge = rows - 1 if d == 0 else 0
-            ends[layer, s, 2 * d : 2 * d + 1, lanes] = a[edge : edge + 1]
-            ends[layer, s, 2 * d + 1 : 2 * d + 2, lanes] = b[edge : edge + 1]
+            ends[layer, block, 2 * d : 2 * d + 1, lanes] = a[edge : edge + 1]
+            ends[layer, block, 2 * d + 1 : 2 * d + 2, lanes] = b[edge : edge + 1]
 
     def e_copy(layer, source, d, to):
         return remote(
@@ -719,22 +753,29 @@
         for d in range(1, n_sp):
             launch(e_copy(layer, s, d, lax.rem(s + d, n_sp)))
 
-    def states(layer):
+    def ends_pair(to_half):
+        here = ends.at[0, pl.ds(2 * to_half, 2)]
+        return remote(here, here, e_send.at[0, 0], e_recv.at[0, 0], "sp", far_mid)
+
+    def gather_ends(layer):
         for d in range(1, n_sp):
             source = lax.rem(s + d, n_sp)
             e_copy(layer, source, d, source).wait_recv()
+
+    def states(layer, k=0):
+        block = end if k else s
         forward = jnp.zeros((1, channels), jnp.float32)
         backward = forward
         for step in range(n_sp - 1):
             forward = jnp.where(
-                step < s, ends[layer, step, 0:1] * forward + ends[layer, step, 1:2], forward
+                step < block, ends[layer, step, 0:1] * forward + ends[layer, step, 1:2], forward
             )
             back = n_sp - 1 - step
             backward = jnp.where(
-                back > s, ends[layer, back, 2:3] * backward + ends[layer, back, 3:4], backward
-            )
-        state = loc[0] + cum[0] * forward + loc[1] + cum[1] * backward
-        gated[...] = (state * y_act[...]).astype(jnp.bfloat16)
+                back > block, ends[layer, back, 2:3] * backward + ends[layer, back, 3:4], backward
+            )
+        state = loc[k, 0] + cum[k, 0] * forward + loc[k, 1] + cum[k, 1] * backward
+        return (state * y_act[k]).astype(jnp.bfloat16)
 
     def a_copy(layer, k):
         return remote(
@@ -758,6 +799,8 @@
             launch(a_copy(layer, k))
         for k in range(2):
             own[k] = branch(layer, 2 * chips[k] + core)
+        if layer == 0:
+            serve(14, 13)
         a_copy(layer, 0).wait_recv()
         for p in range(pieces):
             here = slice(p * part, (p + 1) * part)
@@ -774,6 +817,7 @@
         new = old[here].astype(jnp.float32) + own[1, here]
         return (new + b_in[layer, here].astype(jnp.float32)).astype(jnp.bfloat16)
 
+    launch(boost_copy(), is_end)
     send_outgoing(2)
     for p in range(pieces):
         launch(guest_copy(p), is_end)
@@ -782,9 +826,8 @@
     send_inward(2)
     for n in range(early):
         launch(own_to_near(2 + n // 2, n % 2), is_mid)
-    full[0, t] = stream[...]
     for layer in range(layers):
-        g_out[layer, s] = out_w[layer]
+        rate[layer] = -RECURRENT_WIDTH * softplus(-logit[layer])
 
     serve(2, 4)
     for p in range(pieces):
@@ -817,119 +860,144 @@
 
     @pl.when(is_mid)
     def _():
-        x = project(0, 1)
-        for n in range(groups):
-            p_out[0, n] = x[:, n * width : (n + 1) * width]
+        x = project(0, 0).astype(jnp.float32)
+        xpad[0, HALO : HALO + rows] = x
+        edge = jnp.zeros((HALO, channels), jnp.float32)
 
         @pl.when(half == 0)
         def _():
-            xpad[0, 0:HALO] = x[rows - HALO :].astype(jnp.float32)
+            xpad[guest, 0:HALO] = edge
+            xpad[guest, HALO + rows : 2 * HALO + rows] = x[:HALO]
 
         @pl.when(half == 1)
         def _():
-            xpad[0, HALO + rows : 2 * HALO + rows] = x[:HALO].astype(jnp.float32)
-
-    for n in range(groups):
-        launch(p_copy(0, n), is_mid)
+            xpad[guest, 0:HALO] = x[rows - HALO :]
+            xpad[guest, HALO + rows : 2 * HALO + rows] = edge
+
+    launch(halo_right(0), s == 1)
+    launch(halo_left(0), s == 2)
 
     @pl.when(is_mid)
     def _():
-        xpad[0, HALO : HALO + rows] = project(0, 0).astype(jnp.float32)
-
-    launch(halo_right(0), is_mid)
-    launch(halo_left(0), is_mid)
+        x = project(0, 1).astype(jnp.float32)
+        xpad[guest, HALO : HALO + rows] = x
+
+        @pl.when(half == 0)
+        def _():
+            xpad[0, 0:HALO] = x[rows - HALO :]
+
+        @pl.when(half == 1)
+        def _():
+            xpad[0, HALO + rows : 2 * HALO + rows] = x[:HALO]
+
+        boost_copy().wait_recv()
+
     serve(8, 8)
     send_outgoing(4)
+    for n in range(groups):
+        pl.when(is_mid)(functools.partial(recurrences, 0, n, 1))
+        serve(8 + (n + 2) // 3)
+
+    @pl.when(s == 2)
+    def _():
+        halo_right(0).wait_recv()
+
+    @pl.when(s == 1)
+    def _():
+        halo_left(0).wait_recv()
+
+    for n in range(groups):
+        serve((9, 10, 11)[n])
+        pl.when(is_mid)(functools.partial(recurrences, 0, n))
+    launch(ends_pair(half), is_mid)
+    landed(1)
+
+    @pl.when(is_mid)
+    def _():
+        y_act[1] = jax.nn.gelu(project(1, 1).astype(jnp.float32))
+
+    serve(12, 8)
+
+    @pl.when(is_mid)
+    def _():
+        y_act[0] = jax.nn.gelu(project(1, 0).astype(jnp.float32))
+        ends_pair(1 - half).wait_recv()
+        x = states(0, 1)
+        for n in range(groups):
+            p_out[n] = x[:, n * width : (n + 1) * width]
+
+    for n in range(groups):
+        launch(p_copy(n), is_mid)
+
+    @pl.when(is_mid)
+    def _():
+        gated[...] = states(0)
+
+    serve(12, 12)
+
+    send_outgoing(len(outgoing))
 
     @pl.when(is_end)
     def _():
         for n in range(groups):
-            p_copy(0, n).wait_recv()
-            xpad[0, HALO : HALO + rows, n * width : (n + 1) * width] = p_in[0, n].astype(
-                jnp.float32
-            )
+            p_copy(n).wait_recv()
+            gated[:, n * width : (n + 1) * width] = p_in[n]
 
     for layer in range(layers):
         wx, wy, wo = 3 * layer, 3 * layer + 1, 3 * layer + 2
+        final = layer + 1 == layers
         if layer > 0:
             for p in range(pieces):
                 hand_on(layer, p)
-                serve(4 * wx + 6 + 2 * p // pieces, 4 * wx + 6 + 2 * p // pieces)
+                if layer == 1:
+                    serve((20, 20, 21, 22)[4 * p // pieces], (17, 18, 19, 20)[4 * p // pieces])
             gathered(layer)
             normalise(layer, layer, 0)
             landed(wx)
             xpad[layer, HALO : HALO + rows] = project(wx, 0).astype(jnp.float32)
             launch(halo_right(layer), s < last)
             launch(halo_left(layer), s > 0)
-            serve(4 * wx + 11, 4 * wx + 9)
-
-        @pl.when((s > 0) if layer > 0 else (s >= 2))
-        def _():
-            halo_right(layer).wait_recv()
-
-        @pl.when(s == 0)
-        def _():
-            xpad[layer, 0:HALO] = jnp.zeros((HALO, channels), jnp.float32)
-
-        @pl.when((s < last) if layer > 0 else (s < 2))
-        def _():
-            halo_left(layer).wait_recv()
-
-        @pl.when(s == last)
-        def _():
-            xpad[layer, HALO + rows : 2 * HALO + rows] = jnp.zeros((HALO, channels), jnp.float32)
-
-        for n in range(groups):
-            recurrences(layer, n)
-            if layer == 0:
-                serve(4 * wo + n)
-            else:
-                serve(4 * wx + 12)
-        send_ends(layer)
-        if layer == 0:
-            send_outgoing(4)
-            serve(4 * wo + 4, 4 * wo + 2)
-        if layer == layers - 1:
-            serve(4 * weights, 24)
-        landed(wy)
-        if layer == 0:
-            @pl.when(is_mid)
+            if final:
+                serve((24, 22)[0], (24, 22)[1])
+
+            @pl.when(s > 0)
             def _():
-                y = project(wy, 1)
-                for n in range(groups):
-                    p_out[1, n] = y[:, n * width : (n + 1) * width]
+                halo_right(layer).wait_recv()
+
+            @pl.when(s == 0)
+            def _():
+                xpad[layer, 0:HALO] = jnp.zeros((HALO, channels), jnp.float32)
+
+            @pl.when(s < last)
+            def _():
+                halo_left(layer).wait_recv()
+
+            @pl.when(s == last)
+            def _():
+                xpad[layer, HALO + rows : 2 * HALO + rows] = jnp.zeros(
+                    (HALO, channels), jnp.float32
+                )
 
             for n in range(groups):
-                launch(p_copy(1, n), is_mid)
-
-            @pl.when(is_mid)
-            def _():
-                y_act[...] = jax.nn.gelu(project(wy, 0).astype(jnp.float32))
-
-            serve(4 * wo + 4, 4 * wo + 4)
-
-            @pl.when(is_end)
-            def _():
-                for n in range(groups):
-                    p_copy(1, n).wait_recv()
-                    y_act[:, n * width : (n + 1) * width] = jax.nn.gelu(
-                        p_in[1, n].astype(jnp.float32)
-                    )
-        else:
-            y_act[...] = jax.nn.gelu(project(wy, 0).astype(jnp.float32))
-        states(layer)
+                recurrences(layer, n)
+            send_ends(layer)
+            if final:
+                serve(4 * weights, 24)
+            landed(wy)
+            y_act[0] = jax.nn.gelu(project(wy, 0).astype(jnp.float32))
+            gather_ends(layer)
+            gated[...] = states(layer)
         landed(wo)
         project_out(layer)
-        if layer + 1 < layers:
-            for p in range(pieces):
-                serve(4 * wo + 7 + 3 * p // pieces, 4 * wo + 6 + 4 * p // pieces)
-                full[layer + 1, t, p * part : (p + 1) * part] = finish(
-                    layer, p, stream if layer == 0 else full.at[layer, t]
-                )
+        for p in range(pieces):
+            if layer == 0:
+                serve((16, 17, 18, 19)[4 * p // pieces], (14, 15, 16, 17)[4 * p // pieces])
+            new = finish(layer, p, full.at[layer, t])
+            if final:
+                out[p * part : (p + 1) * part] = new
+            else:
+                full[layer + 1, t, p * part : (p + 1) * part] = new
                 spread(layer + 1, p, full.at[layer + 1, t])
-        else:
-            for p in range(pieces):
-                out[p * part : (p + 1) * part] = finish(layer, p, full.at[layer, t])
 
     for copy, cond in started:
         if cond is None:
@@ -956,25 +1024,33 @@
         width = blocks.shape[-1]
         bf, f32, dma = jnp.bfloat16, jnp.float32, pltpu.SemaphoreType.DMA
         vmem = pltpu.VMEM
-        rate = -RECURRENT_WIDTH * jax.nn.softplus(-logit)
         if folds(n_grp, n_sp, n_tp, layers, rows, ds, cs, channels):
             weights, groups = 3 * layers, channels // width
             return pl.pallas_call(
                 functools.partial(folded_kernel, n_grp, n_sp, n_tp),
                 out_shape=jax.ShapeDtypeStruct((rows, ds), bf),
-                in_specs=[pl.BlockSpec(memory_space=vmem)] * 9,
+                in_specs=[pl.BlockSpec(memory_space=pl.ANY)] * 9,
                 out_specs=pl.BlockSpec(memory_space=vmem),
                 scratch_shapes=[
+                    vmem(gain.shape, f32),
+                    vmem(conv_w.shape, bf),
+                    vmem(gate_w.shape, bf),
+                    vmem(taps.shape, f32),
+                    vmem(blocks.shape, bf),
+                    vmem(logit.shape, f32),
+                    vmem(boost.shape, f32),
+                    vmem(logit.shape, f32),
+                    dma((8 + layers,)),
                     vmem((layers + 1, n_tp, rows, ds), bf),
                     vmem((2, n_sp, rows, cs), bf),
                     vmem((2 * layers, 3, cs, channels), bf),
                     vmem((layers, n_sp, channels, cs), bf),
-                    vmem((layers, rows + 2 * HALO, channels), f32),
-                    vmem((2, groups, rows, width), bf),
-                    vmem((2, groups, rows, width), bf),
-                    vmem((rows, channels), f32),
+                    vmem((layers + 1, rows + 2 * HALO, channels), f32),
+                    vmem((groups, rows, width), bf),
+                    vmem((groups, rows, width), bf),
                     vmem((2, rows, channels), f32),
-                    vmem((2, rows, channels), f32),
+                    vmem((2, 2, rows, channels), f32),
+                    vmem((2, 2, rows, channels), f32),
                     vmem((layers, n_sp, 8, channels), f32),
                     vmem((rows, channels), bf),
                     vmem((layers, 2, rows, ds), bf),
@@ -988,14 +1064,17 @@
                     dma((weights, 2, 2)),
                     dma((weights, 3, 2)),
                     dma((weights, 3, 4)),
+                    vmem((2, rows), f32),
+                    dma((1,)),
+                    dma((1,)),
                     dma((PIECES,)),
                     dma((PIECES,)),
                     dma((layers + 1, PIECES)),
                     dma((layers + 1, PIECES)),
                     dma((layers + 1, PIECES, 2)),
                     dma((layers + 1, PIECES, 2)),
-                    dma((2, groups)),
-                    dma((2, groups)),
+                    dma((groups,)),
+                    dma((groups,)),
                     dma((layers, 2)),
                     dma((layers, 2)),
                     dma((layers, n_sp)),
@@ -1008,8 +1087,8 @@
                 compiler_params=pltpu.CompilerParams(
                     collective_id=0, has_side_effects=True, vmem_limit_bytes=60 * 1024 * 1024
                 ),
-            )(stream, gain, conv_w, gate_w, out_w, taps, blocks, rate, boost)
-        rate = rate.reshape(-1, channels)
+            )(stream, gain, conv_w, gate_w, out_w, taps, blocks, logit, boost)
+        rate = (-RECURRENT_WIDTH * jax.nn.softplus(-logit)).reshape(-1, channels)
         boost = boost.reshape(-1, rows).T
         return pl.pallas_call(
             functools.partial(kernel, n_grp, n_sp, n_tp),

time: 94.8 us -> 89.9 us (0.948)
  Pallas kernels: 91.6 us -> 88.1 us
  other arithmetic: 1.31 us -> 0 us
    pallas_call x1, Pallas kernels: 91.6 us -> 88.1 us  [local(): pl.pallas_call(functools.partial(folded_kernel, n_grp, n_sp, n_tp), out_s...]
    mul x1 -> x0, other arithmetic: 1.31 us -> none  [local(): rate = -RECURRENT_WIDTH * jax.nn.softplus(-logit)]
where the time goes in v3:
time: 89.9 us; the launch traced here: 89.8 us
  Pallas kernels  88.1 us (98%)
  local copies, waits for them, and re-layouts  1.67 us (2%)
    pallas_call x1, Pallas kernels, local(): pl.pallas_call(functools.partial(folded_kernel, n_grp, n_sp, n_tp), out_s...  88.1 us

profile of v3, /device:TPU:0, one launch (start us, length us, event | category | flops | bytes accessed | tf_op | source)
XLA Modules:
  0.0 89.8 jit_solution(14040220387134947403)
XLA Ops:
  0.0 88.1 %shard_map.91 = bf16[256,512]{1,0:T(8,128)(2,1)} custom-call(bf16[256,512]{1,0:T(8,128)(2,1)} %stream_in.1, f32[2,2048]{1,0:T(2,128)} %gain_in.1, bf16[2,512,384]{2,1,0:T(8,128)(2,1)} %conv_in.1, bf16[2,512,384]{2,1,0:T(8,128)(2,1)} %gate_in.1, bf16[2,384,512]{2,1,0:T(8,128)(2,1)} %out_in.1, f32[2,4,384]{2,1,0:T(4,128)} %taps_in.1, ...), custom_call_target="tpu_custom_call" | custom-call | tf_op jit(solution)/shard_map/pallas_call | solution.py:1029
  88.1 1.7 %copy.11 = bf16[256,512]{1,0:T(8,128)(2,1)} copy(bf16[256,512]{1,0:T(8,128)(2,1)} %shard_map.91) | data formatting | bytes 524288

commit v4 on v3

--- a/solution.py
+++ b/solution.py
@@ -601,11 +601,11 @@
         while end_ticks and end_ticks[0] < end:
             end_tick(end_ticks.pop(0))
 
-    def landed(w):
+    def landed(w, chosen=range(3)):
         serve(4 * w + 4 + LAG, 4 * w + 4 + END_LAG if w >= 2 else 0)
 
         def wait_all():
-            for slot in range(3):
+            for slot in chosen:
                 for i in (2, 3):
                     arrived(w, slot, i)
 
@@ -811,6 +811,41 @@
         a_copy(layer, 1).wait_recv()
         own[1] += a_in[layer, 1].astype(jnp.float32)
 
+    def project_last(layer, w):
+        chips = (1 - chip, chip)
+        theirs = [2 * c + 1 - core for c in chips]
+        ours = [2 * c + core for c in chips]
+
+        def give(k):
+            a_out[layer, k] = branch(layer, theirs[k]).astype(jnp.bfloat16)
+
+        def keep(k):
+            own[k] = branch(layer, ours[k])
+
+        def add():
+            a_copy(layer, 0).wait_recv()
+            b_out[layer] = (own[0] + a_in[layer, 0].astype(jnp.float32)).astype(jnp.bfloat16)
+
+        for k in range(2):
+            pl.when(theirs[k] != far_end)(functools.partial(give, k))
+            launch(a_copy(layer, k), theirs[k] != far_end)
+        for k in range(2):
+            pl.when(ours[k] != far_end)(functools.partial(keep, k))
+        pl.when(ours[0] != far_end)(add)
+        for p in range(pieces):
+            launch(b_copy(layer, p), ours[0] != far_end)
+        landed(w, (2,))
+        for k in range(2):
+            pl.when(theirs[k] == far_end)(functools.partial(give, k))
+            launch(a_copy(layer, k), theirs[k] == far_end)
+        for k in range(2):
+            pl.when(ours[k] == far_end)(functools.partial(keep, k))
+        pl.when(ours[0] == far_end)(add)
+        for p in range(pieces):
+            launch(b_copy(layer, p), ours[0] == far_end)
+        a_copy(layer, 1).wait_recv()
+        own[1] += a_in[layer, 1].astype(jnp.float32)
+
     def finish(layer, p, old):
         here = slice(p * part, (p + 1) * part)
         b_copy(layer, p).wait_recv()
@@ -987,8 +1022,12 @@
             y_act[0] = jax.nn.gelu(project(wy, 0).astype(jnp.float32))
             gather_ends(layer)
             gated[...] = states(layer)
-        landed(wo)
-        project_out(layer)
+        if final:
+            landed(wo, (0, 1))
+            project_last(layer, wo)
+        else:
+            landed(wo)
+            project_out(layer)
         for p in range(pieces):
             if layer == 0:
                 serve((16, 17, 18, 19)[4 * p // pieces], (14, 15, 16, 17)[4 * p // pieces])

time: 89.9 us -> 87.7 us (0.976)
  Pallas kernels: 88.1 us -> 85.9 us
    pallas_call x1, Pallas kernels: 88.1 us -> 85.9 us  [local(): pl.pallas_call(functools.partial(folded_kernel, n_grp, n_sp, n_tp), out_s...]
where the time goes in v4:
time: 87.7 us; the launch traced here: 87.6 us
  Pallas kernels  85.9 us (98%)
  local copies, waits for them, and re-layouts  1.67 us (2%)
    pallas_call x1, Pallas kernels, local(): pl.pallas_call(functools.partial(folded_kernel, n_grp, n_sp, n_tp), out_s...  85.9 us

profile of v4, /device:TPU:0, one launch (start us, length us, event | category | flops | bytes accessed | tf_op | source)
XLA Modules:
  0.0 87.6 jit_solution(14849523463268447359)
XLA Ops:
  0.0 85.9 %shard_map.91 = bf16[256,512]{1,0:T(8,128)(2,1)} custom-call(bf16[256,512]{1,0:T(8,128)(2,1)} %stream_in.1, f32[2,2048]{1,0:T(2,128)} %gain_in.1, bf16[2,512,384]{2,1,0:T(8,128)(2,1)} %conv_in.1, bf16[2,512,384]{2,1,0:T(8,128)(2,1)} %gate_in.1, bf16[2,384,512]{2,1,0:T(8,128)(2,1)} %out_in.1, f32[2,4,384]{2,1,0:T(4,128)} %taps_in.1, ...), custom_call_target="tpu_custom_call" | custom-call | tf_op jit(solution)/shard_map/pallas_call | solution.py:1068
  85.9 1.7 %copy.11 = bf16[256,512]{1,0:T(8,128)(2,1)} copy(bf16[256,512]{1,0:T(8,128)(2,1)} %shard_map.91) | data formatting | bytes 524288

commit v5 on v4

--- a/solution.py
+++ b/solution.py
@@ -843,6 +843,8 @@
         pl.when(ours[0] == far_end)(add)
         for p in range(pieces):
             launch(b_copy(layer, p), ours[0] == far_end)
+        if layer + 1 < layers:
+            serve(14, 13)
         a_copy(layer, 1).wait_recv()
         own[1] += a_in[layer, 1].astype(jnp.float32)
 
@@ -1022,12 +1024,8 @@
             y_act[0] = jax.nn.gelu(project(wy, 0).astype(jnp.float32))
             gather_ends(layer)
             gated[...] = states(layer)
-        if final:
-            landed(wo, (0, 1))
-            project_last(layer, wo)
-        else:
-            landed(wo)
-            project_out(layer)
+        landed(wo, (0, 1))
+        project_last(layer, wo)
         for p in range(pieces):
             if layer == 0:
                 serve((16, 17, 18, 19)[4 * p // pieces], (14, 15, 16, 17)[4 * p // pieces])

time: 87.7 us -> 87.3 us (level)
  no operation moved by 1% of the time
where the time goes in v5:
time: 87.3 us; the launch traced here: 87.1 us
  Pallas kernels  85.5 us (98%)
  local copies, waits for them, and re-layouts  1.67 us (2%)
    pallas_call x1, Pallas kernels, local(): pl.pallas_call(functools.partial(folded_kernel, n_grp, n_sp, n_tp), out_s...  85.5 us

profile of v5, /device:TPU:0, one launch (start us, length us, event | category | flops | bytes accessed | tf_op | source)
XLA Modules:
  0.0 87.1 jit_solution(11509575535894248268)
XLA Ops:
  0.0 85.5 %shard_map.91 = bf16[256,512]{1,0:T(8,128)(2,1)} custom-call(bf16[256,512]{1,0:T(8,128)(2,1)} %stream_in.1, f32[2,2048]{1,0:T(2,128)} %gain_in.1, bf16[2,512,384]{2,1,0:T(8,128)(2,1)} %conv_in.1, bf16[2,512,384]{2,1,0:T(8,128)(2,1)} %gate_in.1, bf16[2,384,512]{2,1,0:T(8,128)(2,1)} %out_in.1, f32[2,4,384]{2,1,0:T(4,128)} %taps_in.1, ...), custom_call_target="tpu_custom_call" | custom-call | tf_op jit(solution)/shard_map/pallas_call | solution.py:1066
  85.5 1.7 %copy.11 = bf16[256,512]{1,0:T(8,128)(2,1)} copy(bf16[256,512]{1,0:T(8,128)(2,1)} %shard_map.91) | data formatting | bytes 524288
